TPU v7x, 32 devices: a whole 2x2x4 slice. The times are simulated.
32 devices in a mesh: rep: 2 (over x), fs: 8 (over z, y), tp: 2 (over core).
Axes of the slice: x: 2, y: 2, z: 4, core: 2. Of those that a mesh axis runs over, the one named last changes fastest.
Arguments:
- tokens: bfloat16 [4096, 2048], P(('rep', 'fs')), may hold values from -6 to 6
- mid_tokens: bfloat16 [4096, 2048], P(('rep', 'fs')), may hold values from -6 to 6
- out_grad: bfloat16 [4096, 2048], P(('rep', 'fs')), may hold values from -6 to 6
- gate_first: bfloat16 [2048, 3072], P('fs', 'tp'), may hold values from -0.125 to 0.125
- up_first: bfloat16 [2048, 3072], P('fs', 'tp'), may hold values from -0.125 to 0.125
- down_first: bfloat16 [3072, 2048], P('tp', 'fs'), may hold values from -0.109375 to 0.109375
- gate_second: bfloat16 [2048, 3072], P('fs', 'tp'), may hold values from -0.125 to 0.125
- up_second: bfloat16 [2048, 3072], P('fs', 'tp'), may hold values from -0.125 to 0.125
- down_second: bfloat16 [3072, 2048], P('tp', 'fs'), may hold values from -0.109375 to 0.109375
Outputs:
- input_grad: bfloat16 [4096, 2048], P(('rep', 'fs'))
- down_grad: float32 [3072, 2048], P('tp', 'fs')
- row_norms: float32 [3072], P('tp')
All inputs are finite; a program needn't handle non-finite values.
Results may differ from a plain program's by a relative error of at most 0.025.
Values may be sent and summed in bfloat16 or wider, within the bound.
A program may use at most 128 MiB of HBM per device.

v0:
```python
import jax
import jax.numpy as jnp
from jax import lax
from jax.sharding import PartitionSpec as P

eps = 1e-06


def gathered(gate_w, up_w, down_w):
    half = gate_w.shape[1] // lax.axis_size("rep")
    start = lax.axis_index("rep") * half
    own = jnp.concatenate(
        [
            lax.dynamic_slice_in_dim(gate_w, start, half, 1),
            lax.dynamic_slice_in_dim(up_w, start, half, 1),
            lax.dynamic_slice_in_dim(down_w, start, half, 0).T,
        ],
        axis=1,
    )
    return lax.all_gather(own, "fs", axis=0, tiled=True)


def half_back(field, fields, carried, carrieds, weights):
    half = weights.shape[1] // 3
    wide = fields.astype(jnp.float32)
    normed_b = (wide * lax.rsqrt(jnp.mean(wide * wide, axis=1, keepdims=True) + eps)).astype(
        jnp.bfloat16
    )
    gates, uppers, downs = (weights[:, i * half : (i + 1) * half] for i in range(3))
    gate = jnp.dot(normed_b, gates, preferred_element_type=jnp.float32)
    upper = jnp.dot(normed_b, uppers, preferred_element_type=jnp.float32)
    back = 0.5 * jnp.dot(carrieds, downs, preferred_element_type=jnp.float32)
    logistic = jax.nn.sigmoid(gate)
    activated = gate * logistic
    hidden = (activated * upper).astype(jnp.bfloat16)
    d_gate = (back * upper * logistic * (1.0 + gate * (1.0 - logistic))).astype(jnp.bfloat16)
    d_up = (back * activated).astype(jnp.bfloat16)
    dims = (((1,), (1,)), ((), ()))
    partial_sum = lax.dot_general(d_gate, gates, dims, preferred_element_type=jnp.float32)
    partial_sum = partial_sum + lax.dot_general(
        d_up, uppers, dims, preferred_element_type=jnp.float32
    )
    partial_sum = partial_sum.astype(jnp.bfloat16)
    n = field.shape[0]
    reps = lax.axis_size("rep")
    me = lax.axis_index("rep")
    total = lax.dynamic_slice_in_dim(partial_sum, me * n, n, 0).astype(jnp.float32)
    for k in range(1, reps):
        other = lax.rem(me + k, reps)
        sent = lax.dynamic_slice_in_dim(partial_sum, other * n, n, 0)
        got = lax.ppermute(sent, "rep", [(i, (i + k) % reps) for i in range(reps)])
        total = total + got.astype(jnp.float32)
    d_normed = lax.psum(total.astype(jnp.bfloat16), "tp").astype(jnp.float32)
    own = field.astype(jnp.float32)
    scale = lax.rsqrt(jnp.mean(own * own, axis=1, keepdims=True) + eps)
    normed = own * scale
    d_field = carried.astype(jnp.float32) + scale * (
        d_normed - normed * jnp.mean(d_normed * normed, axis=1, keepdims=True)
    )
    return (d_field.astype(jnp.bfloat16), hidden)


def over_rep(x):
    return lax.all_gather(x, "rep", axis=0, tiled=True)


def on_device(
    tokens,
    mid_tokens,
    out_grad,
    gate_first,
    up_first,
    down_first,
    gate_second,
    up_second,
    down_second,
):
    second = gathered(gate_second, up_second, down_second)
    first = gathered(gate_first, up_first, down_first)
    mid_grad, _ = half_back(mid_tokens, over_rep(mid_tokens), out_grad, over_rep(out_grad), second)
    mid_grads = over_rep(mid_grad)
    d_input, hidden = half_back(tokens, over_rep(tokens), mid_grad, mid_grads, first)
    partial = lax.dot_general(
        mid_grads, hidden, (((0,), (0,)), ((), ())), preferred_element_type=jnp.float32
    )
    shard = lax.psum_scatter(
        (0.5 * partial).astype(jnp.bfloat16), "fs", scatter_dimension=0, tiled=True
    )
    grad = lax.all_gather(shard, "rep", axis=1, tiled=True).astype(jnp.float32)
    norms = lax.psum(jnp.sum(grad * grad, axis=0), "fs")
    return (d_input, grad.T, norms)


def solution(mesh):
    placed = (
        P(("rep", "fs"), None),
        P(("rep", "fs"), None),
        P(("rep", "fs"), None),
        P("fs", "tp"),
        P("fs", "tp"),
        P("tp", "fs"),
        P("fs", "tp"),
        P("fs", "tp"),
        P("tp", "fs"),
    )
    return jax.shard_map(
        on_device,
        mesh=mesh,
        in_specs=placed,
        out_specs=(P(("rep", "fs"), None), P("tp", "fs"), P("tp")),
        check_vma=False,
    )
```

profile of v0, /device:TPU:0, one launch (start us, length us, event | category | flops | bytes accessed | tf_op | source)
XLA Modules:
  0.0 675.1 jit_solution(365070415602245520)
XLA Ops:
  7.2 0.7 all-gather.11.cloned.1.call-update
  8.0 1.2 constant_dynamic-slice_fusion.4
  9.5 1.1 pad_maximum_fusion
  10.7 0.7 all-gather.9.cloned.1.call-update
  11.5 33.9 %all-gather.11.cloned.1.call-done = bf16[512,2048]{1,0:T(8,128)(2,1)} async-done(((bf16[256,2048]{1,0:T(8,128)(2,1)}), bf16[512,2048]{1,0:T(8,128)(2,1)}) %all-gather.11.cloned.1.call-update) | async-done | bytes 2097168 | tf_op jit(solution)/shard_map/all_gather | solution.py:64
  45.4 2.2 fusion
  47.6 138.2 %all-gather.7.cloned.1.call-done = bf16[2048,2304]{0,1:T(8,128)(2,1)} async-done(((bf16[256,2304]{0,1:T(8,128)(2,1)}), bf16[2048,2304]{0,1:T(8,128)(2,1)}) %all-gather.7.cloned.1.call-update) | async-done | bytes 9437200 | tf_op jit(solution)/shard_map/all_gather | solution.py:20
  185.8 4.9 fusion.17
  190.7 27.9 %all-gather.9.cloned.1.call-done = bf16[512,2048]{1,0:T(8,128)(2,1)} async-done(((bf16[256,2048]{1,0:T(8,128)(2,1)}), bf16[512,2048]{1,0:T(8,128)(2,1)}) %all-gather.9.cloned.1.call-update) | async-done | bytes 2097168 | tf_op jit(solution)/shard_map/all_gather | solution.py:64
  218.6 5.5 fusion.42
  224.1 9.8 %fusion.15 = f32[512,2048]{1,0:T(8,128)} fusion(bf16[2048,2304]{0,1:T(8,128)(2,1)} %all-gather.7.cloned.1.call-done, f32[768,512]{1,0:T(8,128)} %fusion.42, f32[512,768]{0,1:T(8,128)} %fusion.17, bf16[512,2048]{1,0:T(8,128)(2,1)S(1)} %copy-done.8, f32[512]{0:T(512)S(1)} %add_rsqrt_fusion.1), kind=kOutput, calls=%fused_computation.22 | convolution fusion | flops 3228303360 | bytes 15730688 | tf_op jit(solution)/shard_map/dot_general | solution.py:39
  233.9 6.0 add_convert_fusion.1
  239.9 1.0 constant_dynamic-slice_fusion.3
  240.9 0.4 collective-permute-start
  241.3 24.7 %collective-permute-done = bf16[256,2048]{1,0:T(8,128)(2,1)} collective-permute-done((bf16[256,2048]{1,0:T(8,128)(2,1)}, bf16[256,2048]{1,0:T(8,128)(2,1)}, u32[]{:S(2)}, u32[]{:S(2)}) %collective-permute-start) | collective-permute-done | bytes 1048608 | tf_op jit(solution)/shard_map/ppermute | solution.py:51
  266.0 2.6 add_convert_fusion.3
  268.6 0.5 all-gather.17.cloned.1.call-update
  269.2 1.2 constant_dynamic-slice_fusion.1
  270.8 1.1 pad_maximum_fusion.1
  272.0 0.4 copy-done.2
  272.4 0.3 fusion.24
  272.7 15.5 %all-reduce.3.cloned.1.call-done = bf16[256,2048]{1,0:T(8,128)(2,1)} async-done(((bf16[256,2048]{1,0:T(8,128)(2,1)}), bf16[256,2048]{1,0:T(8,128)(2,1)}) %all-reduce.3.cloned.1.call-update) | async-done | bytes 1048592 | tf_op jit(solution)/shard_map/psum | solution.py:53
  288.2 1.8 fusion.25
  290.0 1.6 fusion.28
  291.6 0.2 all-reduce.5.cloned.1.call-start
  291.9 32.0 %all-gather.17.cloned.1.call-done = bf16[512,2048]{1,0:T(8,128)(2,1)} async-done(((bf16[256,2048]{1,0:T(8,128)(2,1)}), bf16[512,2048]{1,0:T(8,128)(2,1)}) %all-gather.17.cloned.1.call-update) | async-done | bytes 2097168 | tf_op jit(solution)/shard_map/all_gather | solution.py:64
  323.9 2.2 fusion.2
  326.1 138.0 %all-gather.15.cloned.1.call-done = bf16[2048,2304]{0,1:T(8,128)(2,1)} async-done(((bf16[256,2304]{0,1:T(8,128)(2,1)}), bf16[2048,2304]{0,1:T(8,128)(2,1)}) %all-gather.15.cloned.1.call-update) | async-done | bytes 9437200 | tf_op jit(solution)/shard_map/all_gather | solution.py:20
  464.1 4.9 fusion.10
  469.0 5.2 fusion.13
  474.3 23.3 %all-gather.13.cloned.1.call-done = bf16[512,2048]{1,0:T(8,128)(2,1)} async-done(((bf16[256,2048]{1,0:T(8,128)(2,1)}), bf16[512,2048]{1,0:T(8,128)(2,1)}) %all-gather.13.cloned.1.call-update) | async-done | bytes 2097168 | tf_op jit(solution)/shard_map/all_gather | solution.py:64
  497.5 4.5 fusion.45
  502.0 4.1 fusion.8
  506.2 4.0 add_convert_fusion
  510.2 0.4 collective-permute-start.1
  510.7 24.4 %collective-permute-done.1 = bf16[256,2048]{1,0:T(8,128)(2,1)S(1)} collective-permute-done((bf16[256,2048]{1,0:T(8,128)(2,1)S(1)}, bf16[256,2048]{1,0:T(8,128)(2,1)S(1)}, u32[]{:S(2)}, u32[]{:S(2)}) %collective-permute-start.1) | collective-permute-done | bytes 1048608 | tf_op jit(solution)/shard_map/ppermute | solution.py:51
  535.1 1.4 add_convert_fusion.2
  536.5 0.3 reduce-scatter.2.cloned.1.call-start
  536.7 5.5 multiply_convert_fusion
  542.3 1.2 copy-done.3
  543.5 0.3 fusion.29
  543.8 12.2 %all-reduce.5.cloned.1.call-done = bf16[256,2048]{1,0:T(8,128)(2,1)} async-done(((bf16[256,2048]{1,0:T(8,128)(2,1)}), bf16[256,2048]{1,0:T(8,128)(2,1)}) %all-reduce.5.cloned.1.call-update) | async-done | bytes 1048592 | tf_op jit(solution)/shard_map/psum | solution.py:53
  556.0 1.8 fusion.30
  557.9 1.6 fusion.33
  559.5 75.6 %reduce-scatter.2.cloned.1.call-done = bf16[256,768]{1,0:T(8,128)(2,1)} async-done(((bf16[2048,768]{1,0:T(8,128)(2,1)}), bf16[256,768]{1,0:T(8,128)(2,1)}) %reduce-scatter.2.cloned.1.call-update) | async-done | bytes 393232 | tf_op jit(solution)/shard_map/reduce_scatter | solution.py:86
  635.1 11.0 %all_gather.27 = bf16[256,1536]{1,0:T(8,128)(2,1)S(1)} all-gather(bf16[256,768]{1,0:T(8,128)(2,1)} %reduce-scatter.2.cloned.1.call-done), channel_id=1, replica_groups=mesh['rep'=2,'fs'=8,'tp'=2] {'rep'}, dimensions={1}, use_global_device_ids=true | all-gather | bytes 1179648 | tf_op jit(solution)/shard_map/all_gather | solution.py:89
  646.5 1.6 copy.25
  648.1 20.5 %psum.23 = f32[1536]{0:T(1024)} all-reduce(f32[1536]{0:T(1024)S(1)} %fusion.34), channel_id=1, replica_groups=mesh['rep'=2,'fs'=8,'tp'=2] {'fs'}, use_global_device_ids=true, to_apply=%region_10.0 | all-reduce | flops 1536 | bytes 12288 | tf_op jit(solution)/shard_map/psum | solution.py:90
  (54 shorter events, 1.7 us)
Async XLA Ops:
  7.2 2.3 copy-start
  7.2 38.2 %all-gather.11.cloned.1.call-start = ((), (), s32[]{:S(2)}) async-start(), calls=%async_computation.3 | async-start | bytes 3145728 | tf_op jit(solution)/shard_map/all_gather | solution.py:64
  7.9 177.9 %all-gather.7.cloned.1.call-start = ((), (), s32[]{:S(2)}) async-start(), calls=%async_computation.1 | async-start | bytes 10616832 | tf_op jit(solution)/shard_map/all_gather | solution.py:20
  10.7 208.0 %all-gather.9.cloned.1.call-start = ((), (), s32[]{:S(2)}) async-start(), calls=%async_computation.2 | async-start | bytes 3145728 | tf_op jit(solution)/shard_map/all_gather | solution.py:64
  11.4 276.8 %all-reduce.3.cloned.1.call-start = ((), (), s32[]{:S(2)}) async-start(), calls=%async_computation.4 | async-start | bytes 2097152 | tf_op jit(solution)/shard_map/psum | solution.py:53
  45.4 140.4 %copy-start.8 = (bf16[512,2048]{1,0:T(8,128)(2,1)S(1)}, bf16[512,2048]{1,0:T(8,128)(2,1)}, u32[]{:S(2)}) copy-start(bf16[512,2048]{1,0:T(8,128)(2,1)} %all-gather.11.cloned.1.call-done) | copy-start | bytes 6291460
  240.9 25.1 %collective-permute-start = (bf16[256,2048]{1,0:T(8,128)(2,1)}, bf16[256,2048]{1,0:T(8,128)(2,1)}, u32[]{:S(2)}, u32[]{:S(2)}) collective-permute-start(bf16[256,2048]{1,0:T(8,128)(2,1)} %constant_dynamic-slice_fusion.3), channel_id=1, source_target_pairs={{0,16},{16,0},{1,17},{17,1},{2,18},{18,2},{3,19},{19,3},{4,20},{20... | collective-permute-start | bytes 3145736 | tf_op jit(solution)/shard_map/ppermute | solution.py:51
  268.6 2.2 copy-start.10
  268.6 55.3 %all-gather.17.cloned.1.call-start = ((), (), s32[]{:S(2)}) async-start(), calls=%async_computation.7 | async-start | bytes 3145728 | tf_op jit(solution)/shard_map/all_gather | solution.py:64
  269.2 194.9 %all-gather.15.cloned.1.call-start = ((), (), s32[]{:S(2)}) async-start(), calls=%async_computation.6 | async-start | bytes 10616832 | tf_op jit(solution)/shard_map/all_gather | solution.py:20
  270.8 1.7 copy-start.2
  271.9 18.1 %copy-start.7 = (bf16[256,2048]{1,0:T(8,128)(2,1)S(1)}, bf16[256,2048]{1,0:T(8,128)(2,1)}, u32[]{:S(2)}) copy-start(bf16[256,2048]{1,0:T(8,128)(2,1)} %param.11) | copy-start | bytes 3145732
  271.9 225.6 %all-gather.13.cloned.1.call-start = ((), (), s32[]{:S(2)}) async-start(), calls=%async_computation.5 | async-start | bytes 3145728 | tf_op jit(solution)/shard_map/all_gather | solution.py:64
  288.2 1.8 copy-start.5
  291.6 264.4 %all-reduce.5.cloned.1.call-start = ((), (), s32[]{:S(2)}) async-start(), calls=%async_computation.8 | async-start | bytes 2097152 | tf_op jit(solution)/shard_map/psum | solution.py:53
  323.9 140.2 %copy-start.9 = (bf16[512,2048]{1,0:T(8,128)(2,1)S(1)}, bf16[512,2048]{1,0:T(8,128)(2,1)}, u32[]{:S(2)}) copy-start(bf16[512,2048]{1,0:T(8,128)(2,1)} %all-gather.17.cloned.1.call-done) | copy-start | bytes 6291460
  474.3 27.7 %copy-start.12 = (f32[512,768]{0,1:T(8,128)S(1)}, f32[512,768]{0,1:T(8,128)}, u32[]{:S(2)}) copy-start(f32[512,768]{0,1:T(8,128)} %fusion.10) | copy-start | bytes 4718596
  497.5 4.5 copy-start.13
  510.2 26.5 %copy-start.11 = (bf16[512,2048]{1,0:T(8,128)(2,1)S(1)}, bf16[512,2048]{1,0:T(8,128)(2,1)}, u32[]{:S(2)}) copy-start(bf16[512,2048]{1,0:T(8,128)(2,1)} %all-gather.13.cloned.1.call-done) | copy-start | bytes 6291460
  510.2 24.8 %collective-permute-start.1 = (bf16[256,2048]{1,0:T(8,128)(2,1)S(1)}, bf16[256,2048]{1,0:T(8,128)(2,1)S(1)}, u32[]{:S(2)}, u32[]{:S(2)}) collective-permute-start(bf16[256,2048]{1,0:T(8,128)(2,1)S(1)} %constant_dynamic-slice_fusion), channel_id=1, source_target_pairs={{0,16},{16,0},{1,17},{17,1},{2,18},{18,2},{3,19},{19,3},{4,20},{20... | collective-permute-start | bytes 3145736 | tf_op jit(solution)/shard_map/ppermute | solution.py:51
  536.5 98.7 %reduce-scatter.2.cloned.1.call-start = ((), (), s32[]{:S(2)}) async-start(), calls=%async_computation.9 | async-start | bytes 3538944 | tf_op jit(solution)/shard_map/reduce_scatter | solution.py:86
  542.2 1.3 copy-start.3
  543.5 14.4 %copy-start.4 = (bf16[256,2048]{1,0:T(8,128)(2,1)S(1)}, bf16[256,2048]{1,0:T(8,128)(2,1)}, u32[]{:S(2)}) copy-start(bf16[256,2048]{1,0:T(8,128)(2,1)} %fusion.28) | copy-start | bytes 3145732
  556.0 1.8 copy-start.6
  646.1 22.4 %copy-start.1 = (bf16[1536,256]{1,0:T(8,128)(2,1)S(1)}, bf16[1536,256]{1,0:T(8,128)(2,1)}, u32[]{:S(2)}) copy-start(bf16[1536,256]{1,0:T(8,128)(2,1)} %param.17) | copy-start | bytes 2359300
Sparse Core Ops, SparseCore 0:
  9.5 35.8 all-gather.10
  48.0 137.7 all-gather.6
  187.3 31.2 all-gather.8
  268.7 19.4 all-reduce.2
  289.5 34.2 all-gather.16
  326.3 137.7 all-gather.14
  466.2 31.2 all-gather.12
  536.6 19.4 all-reduce.4
  559.6 75.4 reduce-scatter.1
where the time goes:
time: 676 us; the launch traced here: 675 us
  waiting for transfers between devices  548 us (81%)
  matrix products  54.4 us (8%)
  blocking collectives  31.5 us (5%)
  other arithmetic  18.4 us (3%)
  between operations  14.1 us (2%)
  local copies, waits for them, and re-layouts  7.56 us (1%)
    all_gather x2, waiting for transfers between devices, gathered(): return lax.all_gather(own, 'fs', axis=0, tiled=True)  276 us
    all_gather x4, waiting for transfers between devices, over_rep(): return lax.all_gather(x, 'rep', axis=0, tiled=True)  117 us
    reduce_scatter x1, waiting for transfers between devices, on_device(): lax.psum_scatter((0.5 * partial).astype(jnp.bfloat16), 'fs', scatter_dime...  75.6 us
    ppermute x2, waiting for transfers between devices, half_back(): got = lax.ppermute(sent, 'rep', [(i, (i + k) % reps) for i in range(reps)])  49.1 us
    psum x2, waiting for transfers between devices, half_back(): d_normed = lax.psum(total.astype(jnp.bfloat16), 'tp').astype(jnp.float32)  27.7 us
    psum x1, blocking collectives, on_device(): norms = lax.psum(jnp.sum(grad * grad, axis=0), 'fs')  20.5 us
    dot_general x2, matrix products, half_back(): lax.dot_general(d_gate, gates, dims, preferred_element_type=jnp.float32)  13.9 us
  transfers between devices with their start and end apart: 11, of which 11 were waited for; matrix products, arithmetic and copies ran while one was open for 6% of the time, Pallas kernels for 0%

commit v1 on v0

--- a/solution.py
+++ b/solution.py
@@ -61,7 +61,9 @@
 
 
 def over_rep(x):
-    return lax.all_gather(x, "rep", axis=0, tiled=True)
+    return jnp.concatenate(
+        lax.all_to_all(jnp.stack([x] * lax.axis_size("rep")), "rep", 0, 0), axis=0
+    )
 
 
 def on_device(

time: 676 us -> 554 us (0.82)
  waiting for transfers between devices: 548 us -> 396 us
  starting transfers between devices: 1.53 us -> 21.3 us
  other arithmetic: 18.4 us -> 25.2 us
    all_gather x4 -> x0, waiting for transfers between devices: 117 us -> none  [over_rep(): return lax.all_gather(x, 'rep', axis=0, tiled=True)]
    all_gather x2, waiting for transfers between devices: 276 us -> 218 us  [gathered(): return lax.all_gather(own, 'fs', axis=0, tiled=True)]
    all_to_all x0 -> x4, waiting for transfers between devices: none -> 45.8 us  [over_rep(): lax.all_to_all(jnp.stack([x] * lax.axis_size('rep')), 'rep', 0, 0)]
    all_to_all x0 -> x4, starting transfers between devices: none -> 17.8 us  [over_rep(): lax.all_to_all(jnp.stack([x] * lax.axis_size('rep')), 'rep', 0, 0)]
    psum x2, waiting for transfers between devices: 27.7 us -> 10.6 us  [half_back(): d_normed = lax.psum(total.astype(jnp.bfloat16), 'tp').astype(jnp.float32)]
    another operation x0 -> x4, other arithmetic: none -> 7.53 us  [over_rep(): jnp.stack([x] * lax.axis_size('rep'))]
  transfers between devices with their start and end apart: 11 -> 11, of which waited for: 11 -> 8; matrix products, arithmetic and copies ran while one was open for 6% -> 8% of each run, Pallas kernels for 0% -> 0%
where the time goes in v1:
time: 554 us; the launch traced here: 553 us
  waiting for transfers between devices  396 us (71%)
  matrix products  56.5 us (10%)
  blocking collectives  31.5 us (6%)
  other arithmetic  25.2 us (5%)
  starting transfers between devices  21.3 us (4%)
  between operations  14 us (3%)
  local copies, waits for them, and re-layouts  8.77 us (2%)
    all_gather x2, waiting for transfers between devices, gathered(): return lax.all_gather(own, 'fs', axis=0, tiled=True)  218 us
    reduce_scatter x1, waiting for transfers between devices, on_device(): lax.psum_scatter((0.5 * partial).astype(jnp.bfloat16), 'fs', scatter_dime...  75.5 us
    all_to_all x4, waiting for transfers between devices, over_rep(): lax.all_to_all(jnp.stack([x] * lax.axis_size('rep')), 'rep', 0, 0)  45.8 us
    ppermute x2, waiting for transfers between devices, half_back(): got = lax.ppermute(sent, 'rep', [(i, (i + k) % reps) for i in range(reps)])  45.6 us
    psum x1, blocking collectives, on_device(): norms = lax.psum(jnp.sum(grad * grad, axis=0), 'fs')  20.5 us
    all_to_all x4, starting transfers between devices, over_rep(): lax.all_to_all(jnp.stack([x] * lax.axis_size('rep')), 'rep', 0, 0)  17.8 us
    dot_general x2, matrix products, half_back(): lax.dot_general(d_gate, gates, dims, preferred_element_type=jnp.float32)  14 us
  transfers between devices with their start and end apart: 11, of which 8 were waited for; matrix products, arithmetic and copies ran while one was open for 8% of the time, Pallas kernels for 0%

profile of v1, /device:TPU:0, one launch (start us, length us, event | category | flops | bytes accessed | tf_op | source)
XLA Modules:
  0.0 553.0 jit_solution(5039791954245912608)
XLA Ops:
  7.2 1.2 constant_dynamic-slice_fusion.4
  8.9 1.1 pad_maximum_fusion.4
  10.5 1.5 pad_maximum_fusion.1
  12.0 4.2 all-to-all-start.1
  16.2 3.1 pad_maximum_fusion
  19.3 22.8 %all-to-all-done.1 = bf16[2,256,2048]{2,1,0:T(8,128)(2,1)S(1)} async-done(((bf16[2,256,2048]{2,1,0:T(8,128)(2,1)}), bf16[2,256,2048]{2,1,0:T(8,128)(2,1)S(1)}, u32[]{:S(2)}, u32[]{:S(2)}) %all-to-all-start.1) | async-done | bytes 2097184 | tf_op jit(solution)/shard_map/all_to_all | solution.py:65
  42.1 4.8 all-to-all-start
  46.9 0.5 multiply_reduce_fusion.1
  47.4 1.8 fusion.1
  49.2 101.9 %all-gather.3.cloned.1.call-done = bf16[2048,2304]{0,1:T(8,128)(2,1)} async-done(((bf16[256,2304]{0,1:T(8,128)(2,1)}), bf16[2048,2304]{0,1:T(8,128)(2,1)}) %all-gather.3.cloned.1.call-update) | async-done | bytes 9437200 | tf_op jit(solution)/shard_map/all_gather | solution.py:20
  151.1 5.5 fusion.15
  156.6 5.7 %fusion.36 = f32[512,768]{1,0:T(8,128)} fusion(bf16[512,2048]{1,0:T(8,128)(2,1)} %bitcast.1, bf16[2048,2304]{0,1:T(8,128)(2,1)} %all-gather.3.cloned.1.call-done), kind=kOutput, calls=%fused_computation.64 | convolution fusion | flops 1611005952 | bytes 6815744 | tf_op jit(solution)/shard_map/dot_general | solution.py:32
  162.3 9.9 %fusion.13 = f32[512,2048]{1,0:T(8,128)} fusion(bf16[2048,2304]{0,1:T(8,128)(2,1)} %all-gather.3.cloned.1.call-done, f32[512,768]{1,0:T(8,128)} %fusion.15, f32[512,768]{1,0:T(8,128)} %fusion.36, bf16[512,2048]{1,0:T(8,128)(2,1)S(1)} %copy-done.8), kind=kOutput, calls=%fused_computation.20 | convolution fusion | flops 3225157632 | bytes 15728640 | tf_op jit(solution)/shard_map/dot_general | solution.py:39
  172.1 5.9 %add_convert_fusion.1 = bf16[512,2048]{1,0:T(8,128)(2,1)S(1)} fusion(f32[512,2048]{1,0:T(8,128)} %fusion.13, bf16[2048,2304]{0,1:T(8,128)(2,1)} %all-gather.3.cloned.1.call-done, f32[512,768]{1,0:T(8,128)} %fusion.36, f32[512,768]{1,0:T(8,128)} %fusion.15), kind=kOutput, calls=%fused_computation.7 | convolution fusion | flops 1615069184 | bytes 12582912 | tf_op jit(solution)/shard_map/dot_general | solution.py:40
  178.0 1.0 constant_dynamic-slice_fusion.3
  179.1 1.5 collective-permute-start
  180.6 22.9 %collective-permute-done = bf16[256,2048]{1,0:T(8,128)(2,1)} collective-permute-done((bf16[256,2048]{1,0:T(8,128)(2,1)}, bf16[256,2048]{1,0:T(8,128)(2,1)}, u32[]{:S(2)}, u32[]{:S(2)}) %collective-permute-start) | collective-permute-done | bytes 1048608 | tf_op jit(solution)/shard_map/ppermute | solution.py:51
  203.5 2.6 add_convert_fusion.3
  206.2 1.2 constant_dynamic-slice_fusion.1
  207.7 1.1 dynamic-slice_bitcast_fusion
  208.8 1.1 pad_maximum_fusion.5
  210.0 1.5 pad_maximum_fusion.3
  211.4 3.9 all-to-all-start.3
  215.7 23.1 %all-to-all-done.3 = bf16[2,256,2048]{2,1,0:T(8,128)(2,1)S(1)} async-done(((bf16[2,256,2048]{2,1,0:T(8,128)(2,1)}), bf16[2,256,2048]{2,1,0:T(8,128)(2,1)S(1)}, u32[]{:S(2)}, u32[]{:S(2)}) %all-to-all-start.3) | async-done | bytes 2097184 | tf_op jit(solution)/shard_map/all_to_all | solution.py:65
  238.8 0.5 multiply_reduce_fusion
  239.3 1.8 fusion
  241.1 1.9 fusion.23
  243.0 0.7 fusion.26
  243.6 1.5 pad_maximum_fusion.2
  245.1 4.8 all-to-all-start.2
  250.0 116.3 %all-gather.5.cloned.1.call-done = bf16[2048,2304]{0,1:T(8,128)(2,1)} async-done(((bf16[256,2304]{0,1:T(8,128)(2,1)}), bf16[2048,2304]{0,1:T(8,128)(2,1)}) %all-gather.5.cloned.1.call-update) | async-done | bytes 9437200 | tf_op jit(solution)/shard_map/all_gather | solution.py:20
  366.3 5.5 fusion.8
  371.8 5.5 fusion.11
  377.3 4.5 fusion.39
  381.8 4.2 fusion.6
  386.0 3.8 add_convert_fusion
  389.9 1.6 collective-permute-start.1
  391.5 22.6 %collective-permute-done.1 = bf16[256,2048]{1,0:T(8,128)(2,1)S(1)} collective-permute-done((bf16[256,2048]{1,0:T(8,128)(2,1)S(1)}, bf16[256,2048]{1,0:T(8,128)(2,1)S(1)}, u32[]{:S(2)}, u32[]{:S(2)}) %collective-permute-start.1) | collective-permute-done | bytes 1048608 | tf_op jit(solution)/shard_map/ppermute | solution.py:51
  414.1 1.4 add_convert_fusion.2
  415.8 6.1 %multiply_convert_fusion = bf16[2048,768]{1,0:T(8,128)(2,1)} fusion(bf16[512,2048]{1,0:T(8,128)(2,1)} %bitcast.6, f32[512,768]{1,0:T(8,128)} %fusion.11, f32[512,768]{1,0:T(8,128)} %fusion.8), kind=kOutput, calls=%fused_computation | convolution fusion | flops 1616117760 | bytes 8388608 | tf_op jit(solution)/shard_map/dot_general | solution.py:85
  421.9 1.2 copy-done.4
  423.5 10.6 %all-reduce.5.cloned.1.call-done = bf16[256,2048]{1,0:T(8,128)(2,1)} async-done(((bf16[256,2048]{1,0:T(8,128)(2,1)}), bf16[256,2048]{1,0:T(8,128)(2,1)}) %all-reduce.5.cloned.1.call-update) | async-done | bytes 1048592 | tf_op jit(solution)/shard_map/psum | solution.py:53
  434.1 1.8 fusion.28
  435.9 1.6 fusion.31
  437.5 75.5 %reduce-scatter.2.cloned.1.call-done = bf16[256,768]{1,0:T(8,128)(2,1)} async-done(((bf16[2048,768]{1,0:T(8,128)(2,1)}), bf16[256,768]{1,0:T(8,128)(2,1)}) %reduce-scatter.2.cloned.1.call-update) | async-done | bytes 393232 | tf_op jit(solution)/shard_map/reduce_scatter | solution.py:88
  513.0 11.0 %all_gather.11 = bf16[256,1536]{1,0:T(8,128)(2,1)S(1)} all-gather(bf16[256,768]{1,0:T(8,128)(2,1)} %reduce-scatter.2.cloned.1.call-done), channel_id=1, replica_groups=mesh['rep'=2,'fs'=8,'tp'=2] {'rep'}, dimensions={1}, use_global_device_ids=true | all-gather | bytes 1179648 | tf_op jit(solution)/shard_map/all_gather | solution.py:91
  524.4 1.6 copy.16
  526.0 20.5 %psum.23 = f32[1536]{0:T(1024)} all-reduce(f32[1536]{0:T(1024)S(1)} %fusion.32), channel_id=1, replica_groups=mesh['rep'=2,'fs'=8,'tp'=2] {'fs'}, use_global_device_ids=true, to_apply=%region_10.0 | all-reduce | flops 1536 | bytes 12288 | tf_op jit(solution)/shard_map/psum | solution.py:92
  (52 shorter events, 2.8 us)
Async XLA Ops:
  7.2 1.7 copy-start
  7.2 143.9 %all-gather.3.cloned.1.call-start = ((), (), s32[]{:S(2)}) async-start(), calls=%async_computation.5 | async-start | bytes 10616832 | tf_op jit(solution)/shard_map/all_gather | solution.py:20
  8.8 1.7 copy-start.2
  12.0 30.1 %all-to-all-start.1 = ((bf16[2,256,2048]{2,1,0:T(8,128)(2,1)}), bf16[2,256,2048]{2,1,0:T(8,128)(2,1)S(1)}, u32[]{:S(2)}, u32[]{:S(2)}) async-start(bf16[2,256,2048]{2,1,0:T(8,128)(2,1)} %pad_maximum_fusion.1), calls=%async_computation.1 | async-start | bytes 4194304 | tf_op jit(solution)/shard_map/all_to_all | solution.py:65
  42.1 114.5 %all-to-all-start = ((bf16[2,256,2048]{2,1,0:T(8,128)(2,1)}), bf16[2,256,2048]{2,1,0:T(8,128)(2,1)}, u32[]{:S(2)}, u32[]{:S(2)}) async-start(bf16[2,256,2048]{2,1,0:T(8,128)(2,1)} %pad_maximum_fusion), calls=%async_computation | async-start | bytes 4194304 | tf_op jit(solution)/shard_map/all_to_all | solution.py:65
  46.9 194.2 %all-reduce.3.cloned.1.call-start = ((), (), s32[]{:S(2)}) async-start(), calls=%async_computation.6 | async-start | bytes 2097152 | tf_op jit(solution)/shard_map/psum | solution.py:53
  156.6 5.7 %copy-start.8 = (bf16[512,2048]{1,0:T(8,128)(2,1)S(1)}, bf16[512,2048]{1,0:T(8,128)(2,1)}, u32[]{:S(2)}) copy-start(bf16[512,2048]{1,0:T(8,128)(2,1)} %fusion.1) | copy-start | bytes 6291460
  179.1 24.4 %collective-permute-start = (bf16[256,2048]{1,0:T(8,128)(2,1)}, bf16[256,2048]{1,0:T(8,128)(2,1)}, u32[]{:S(2)}, u32[]{:S(2)}) collective-permute-start(bf16[256,2048]{1,0:T(8,128)(2,1)} %constant_dynamic-slice_fusion.3), channel_id=1, source_target_pairs={{0,16},{16,0},{1,17},{17,1},{2,18},{18,2},{3,19},{19,3},{4,20},{20... | collective-permute-start | bytes 3145736 | tf_op jit(solution)/shard_map/ppermute | solution.py:51
  206.1 160.2 %all-gather.5.cloned.1.call-start = ((), (), s32[]{:S(2)}) async-start(), calls=%async_computation.7 | async-start | bytes 10616832 | tf_op jit(solution)/shard_map/all_gather | solution.py:20
  207.7 2.2 copy-start.3
  211.4 27.3 %all-to-all-start.3 = ((bf16[2,256,2048]{2,1,0:T(8,128)(2,1)}), bf16[2,256,2048]{2,1,0:T(8,128)(2,1)S(1)}, u32[]{:S(2)}, u32[]{:S(2)}) async-start(bf16[2,256,2048]{2,1,0:T(8,128)(2,1)} %pad_maximum_fusion.3), calls=%async_computation.3 | async-start | bytes 4194304 | tf_op jit(solution)/shard_map/all_to_all | solution.py:65
  241.1 1.9 copy-start.5
  241.1 1.9 copy-start.6
  245.1 132.1 %all-to-all-start.2 = ((bf16[2,256,2048]{2,1,0:T(8,128)(2,1)}), bf16[2,256,2048]{2,1,0:T(8,128)(2,1)}, u32[]{:S(2)}, u32[]{:S(2)}) async-start(bf16[2,256,2048]{2,1,0:T(8,128)(2,1)} %pad_maximum_fusion.2), calls=%async_computation.2 | async-start | bytes 4194304 | tf_op jit(solution)/shard_map/all_to_all | solution.py:65
  250.0 184.1 %all-reduce.5.cloned.1.call-start = ((), (), s32[]{:S(2)}) async-start(), calls=%async_computation.8 | async-start | bytes 2097152 | tf_op jit(solution)/shard_map/psum | solution.py:53
  377.3 4.5 copy-start.9
  377.3 4.5 copy-start.10
  389.9 24.2 %collective-permute-start.1 = (bf16[256,2048]{1,0:T(8,128)(2,1)S(1)}, bf16[256,2048]{1,0:T(8,128)(2,1)S(1)}, u32[]{:S(2)}, u32[]{:S(2)}) collective-permute-start(bf16[256,2048]{1,0:T(8,128)(2,1)S(1)} %constant_dynamic-slice_fusion), channel_id=1, source_target_pairs={{0,16},{16,0},{1,17},{17,1},{2,18},{18,2},{3,19},{19,3},{4,20},{20... | collective-permute-start | bytes 3145736 | tf_op jit(solution)/shard_map/ppermute | solution.py:51
  415.5 97.5 %reduce-scatter.2.cloned.1.call-start = ((), (), s32[]{:S(2)}) async-start(), calls=%async_computation.9 | async-start | bytes 3538944 | tf_op jit(solution)/shard_map/reduce_scatter | solution.py:88
  421.9 1.3 copy-start.4
  434.1 1.8 copy-start.7
  524.0 22.5 %copy-start.1 = (bf16[1536,256]{1,0:T(8,128)(2,1)S(1)}, bf16[1536,256]{1,0:T(8,128)(2,1)}, u32[]{:S(2)}) copy-start(bf16[1536,256]{1,0:T(8,128)(2,1)} %param.17) | copy-start | bytes 2359300
Sparse Core Ops, SparseCore 0:
  10.6 140.4 all-gather.2
  206.3 18.4 all-reduce.2
  227.3 138.9 all-gather.4
  415.6 18.4 all-reduce.4
  437.5 75.4 reduce-scatter.1
